TPU v7x, 32 devices: a whole 2x2x4 slice. The times are simulated.
32 devices in a mesh: gr: 2 (over x), fs: 8 (over z, y), tp: 2 (over core).
Axes of the slice: x: 2, y: 2, z: 4, core: 2. Of those that a mesh axis runs over, the one named last changes fastest.
Arguments:
- prompt_tokens: bfloat16 [4608, 2048], P(('gr', 'fs', 'tp')), may hold values from -6 to 6
- up_master: float32 [2048, 8192], P(('gr', 'fs'), 'tp'), may hold values from -0.125 to 0.125
- down_master: float32 [2048, 8192], P(('gr', 'fs'), 'tp'), may hold values from -0.0625 to 0.0625
- norm_gain: float32 [2048], P(('gr', 'fs')), may hold values from 0.1 to 1.9
Outputs:
- sampler_up: bfloat16 [2048, 8192], P(None, ('gr', 'tp'))
- sampler_down: bfloat16 [2048, 8192], P(None, ('gr', 'tp'))
- prompt_out: bfloat16 [4608, 2048], P(('gr', 'fs', 'tp'))
All inputs are finite; a program needn't handle non-finite values.
Results may differ from a plain program's by a relative error of at most 0.009.
Values may be sent and summed in bfloat16 or wider, within the bound.
A program may use at most 128 MiB of HBM per device.

v0:
```python
import jax
import jax.numpy as jnp
from jax import lax
from jax.sharding import PartitionSpec as P


def regroup(matrix, groups, shards):
    block = matrix.shape[0] // (groups * shards)
    shaped = matrix.reshape(shards, groups, block, matrix.shape[1])
    return shaped.transpose(1, 0, 2, 3).reshape(groups * shards * block, matrix.shape[1])


def body(prompt_tokens, up_master, down_master, norm_gain):
    up_local = (norm_gain[:, None] * up_master).astype(jnp.bfloat16)
    down_local = down_master.astype(jnp.bfloat16)
    moved = (
        lax.all_to_all(
            lax.all_to_all(up_local, "tp", split_axis=1, concat_axis=0, tiled=True),
            "gr",
            split_axis=0,
            concat_axis=0,
            tiled=True,
        ),
        lax.all_to_all(
            lax.all_to_all(down_local, "tp", split_axis=1, concat_axis=0, tiled=True),
            "gr",
            split_axis=0,
            concat_axis=0,
            tiled=True,
        ),
    )
    stacked = (
        lax.all_gather(moved[0], "fs", axis=0, tiled=True),
        lax.all_gather(moved[1], "fs", axis=0, tiled=True),
    )
    groups = lax.axis_size("gr")
    shards = lax.axis_size("fs")
    sampler_up = regroup(stacked[0], groups, shards)
    sampler_down = regroup(stacked[1], groups, shards)
    values = prompt_tokens.astype(jnp.float32)
    center = jnp.mean(values, axis=-1, keepdims=True)
    variance = jnp.mean(jnp.square(values - center), axis=-1, keepdims=True)
    normed = ((values - center) * lax.rsqrt(variance + 1e-05)).astype(jnp.bfloat16)
    lifted = jax.nn.relu(
        jnp.dot(
            lax.all_gather(normed, ("gr", "tp"), axis=0, tiled=True),
            sampler_up,
            preferred_element_type=jnp.float32,
        )
    )
    hidden = (lifted * lifted).astype(jnp.bfloat16)
    partial_value = lax.dot_general(
        hidden, sampler_down, (((1,), (1,)), ((), ())), preferred_element_type=jnp.float32
    )
    summed = lax.psum_scatter(
        lax.optimization_barrier(partial_value.astype(jnp.bfloat16))
        .astype(jnp.float32)
        .astype(jnp.bfloat16),
        ("gr", "tp"),
        scatter_dimension=0,
        tiled=True,
    )
    return (sampler_up, sampler_down, summed)


def solution(mesh):
    placed = (
        P(("gr", "fs", "tp"), None),
        P(("gr", "fs"), "tp"),
        P(("gr", "fs"), "tp"),
        P(("gr", "fs")),
    )
    return jax.shard_map(
        body,
        mesh=mesh,
        in_specs=placed,
        out_specs=(P(None, ("gr", "tp")), P(None, ("gr", "tp")), P(("gr", "fs", "tp"), None)),
        check_vma=False,
    )
```

profile of v0, /device:TPU:0, one launch (start us, length us, event | category | flops | bytes accessed | tf_op | source)
XLA Modules:
  0.0 364.8 jit_solution(9255359435102102182)
XLA Ops:
  7.2 0.0 copy-start.2
  7.2 0.0 all-gather.4.cloned.1.call-start
  7.2 1.9 copy.7
  9.1 0.0 copy-done.2
  9.2 0.1 multiply_convert_fusion.1
  9.3 4.6 %all_to_all.50 = bf16[128,2,2048]{0,2,1:T(8,128)(2,1)S(1)} all-to-all(bf16[128,2,2048]{0,2,1:T(8,128)(2,1)S(1)} %bitcast.35), channel_id=1, replica_groups=mesh['gr'=2,'fs'=8,'tp'=2] {'tp'}, dimensions={1} | all-to-all | bytes 2097152 | tf_op jit(solution)/shard_map/all_to_all | solution.py:18
  13.8 0.0 copy-start.1
  13.8 18.0 %all_to_all.51 = bf16[2,128,2048]{1,2,0:T(8,128)(2,1)S(1)} all-to-all(bf16[2,128,2048]{1,2,0:T(8,128)(2,1)S(1)} %bitcast.36), channel_id=1, replica_groups=mesh['gr'=2,'fs'=8,'tp'=2] {'gr'}, dimensions={0} | all-to-all | bytes 2097152 | tf_op jit(solution)/shard_map/all_to_all | solution.py:17
  31.9 1.3 copy.8
  33.2 0.0 all-gather.4.cloned.1.call-update
  33.2 0.0 all-gather.6.cloned.1.call-start
  33.3 0.0 copy-done.1
  33.3 0.7 copy.10
  34.0 4.6 %all_to_all.52 = bf16[128,2,2048]{0,2,1:T(8,128)(2,1)S(1)} all-to-all(bf16[128,2,2048]{0,2,1:T(8,128)(2,1)S(1)} %bitcast.32), channel_id=1, replica_groups=mesh['gr'=2,'fs'=8,'tp'=2] {'tp'}, dimensions={1} | all-to-all | bytes 2097152 | tf_op jit(solution)/shard_map/all_to_all | solution.py:25
  38.6 0.0 copy-start
  38.6 16.7 %all_to_all.53 = bf16[2,128,2048]{1,2,0:T(8,128)(2,1)S(1)} all-to-all(bf16[2,128,2048]{1,2,0:T(8,128)(2,1)S(1)} %bitcast.37), channel_id=1, replica_groups=mesh['gr'=2,'fs'=8,'tp'=2] {'gr'}, dimensions={0} | all-to-all | bytes 2097152 | tf_op jit(solution)/shard_map/all_to_all | solution.py:24
  55.4 1.3 copy.11
  56.7 0.0 all-gather.6.cloned.1.call-update
  56.7 0.0 all-gather.8.cloned.1.call-start
  56.7 0.0 copy-done
  56.7 0.2 convert_reduce_fusion
  56.9 0.3 fusion.2
  57.2 1.2 fusion.3
  58.4 0.0 all-gather.8.cloned.1.call-update
  58.4 0.0 reduce-scatter.2.cloned.1.call-start
  58.5 99.9 %all-gather.4.cloned.1.call-done = bf16[2048,2048]{1,0:T(8,128)(2,1)} async-done(((bf16[256,2048]{1,0:T(8,128)(2,1)}), bf16[2048,2048]{1,0:T(8,128)(2,1)}) %all-gather.4.cloned.1.call-update) | async-done | bytes 8388624 | tf_op jit(solution)/shard_map/all_gather | solution.py:33
  158.4 8.4 %copy.9 = bf16[2,8,128,2048]{3,2,1,0:T(8,128)(2,1)} copy(bf16[2,8,128,2048]{3,2,0,1:T(8,128)(2,1)} %bitcast.26) | data formatting | bytes 16777216 | tf_op jit(solution)/shard_map/transpose | solution.py:10
  166.8 116.4 %all-gather.6.cloned.1.call-done = bf16[2048,2048]{1,0:T(8,128)(2,1)} async-done(((bf16[256,2048]{1,0:T(8,128)(2,1)}), bf16[2048,2048]{1,0:T(8,128)(2,1)}) %all-gather.6.cloned.1.call-update) | async-done | bytes 8388624 | tf_op jit(solution)/shard_map/all_gather | solution.py:34
  283.2 8.6 %copy.12 = bf16[2,8,128,2048]{3,2,1,0:T(8,128)(2,1)} copy(bf16[2,8,128,2048]{3,2,0,1:T(8,128)(2,1)} %bitcast.27) | data formatting | bytes 16777216 | tf_op jit(solution)/shard_map/transpose | solution.py:10
  291.8 15.8 %all-gather.8.cloned.1.call-done = bf16[576,2048]{1,0:T(8,128)(2,1)} async-done(((bf16[144,2048]{1,0:T(8,128)(2,1)}), bf16[576,2048]{1,0:T(8,128)(2,1)}) %all-gather.8.cloned.1.call-update) | async-done | bytes 2359312 | tf_op jit(solution)/shard_map/all_gather | solution.py:46
  307.6 17.7 %convolution_convert_fusion = bf16[576,2048]{1,0:T(8,128)(2,1)} fusion(bf16[2048,2048]{1,0:T(8,128)(2,1)} %bitcast.30, bf16[576,2048]{1,0:T(8,128)(2,1)} %all-gather.8.cloned.1.call-done, bf16[2048,2048]{1,0:T(8,128)(2,1)} %bitcast.28), kind=kOutput, calls=%fused_computation.1 | convolution fusion | flops 9668395008 | bytes 21495808 | tf_op jit(solution)/shard_map/dot_general | solution.py:52
  325.3 0.0 reduce-scatter.2.cloned.1.call-update
  325.3 33.0 %reduce-scatter.2.cloned.1.call-done = bf16[144,2048]{1,0:T(8,128)(2,1)} async-done(((bf16[576,2048]{1,0:T(8,128)(2,1)}), bf16[144,2048]{1,0:T(8,128)(2,1)}) %reduce-scatter.2.cloned.1.call-update) | async-done | bytes 589840 | tf_op jit(solution)/shard_map/reduce_scatter | solution.py:55
  (2 shorter events, 0.0 us)
Async XLA Ops:
  7.2 2.0 copy-start.2
  7.2 151.2 %all-gather.4.cloned.1.call-start = ((), (), s32[]{:S(2)}) async-start(), calls=%async_computation.5 | async-start | bytes 9437184 | tf_op jit(solution)/shard_map/all_gather | solution.py:33
  13.8 19.4 %copy-start.1 = (f32[128,4096]{1,0:T(8,128)S(1)}, f32[128,4096]{1,0:T(8,128)}, u32[]{:S(2)}) copy-start(f32[128,4096]{1,0:T(8,128)} %param.6) | copy-start | bytes 6291460
  33.2 249.9 %all-gather.6.cloned.1.call-start = ((), (), s32[]{:S(2)}) async-start(), calls=%async_computation.6 | async-start | bytes 9437184 | tf_op jit(solution)/shard_map/all_gather | solution.py:34
  38.6 18.1 %copy-start = (bf16[144,2048]{1,0:T(8,128)(2,1)S(1)}, bf16[144,2048]{1,0:T(8,128)(2,1)}, u32[]{:S(2)}) copy-start(bf16[144,2048]{1,0:T(8,128)(2,1)} %param.4) | copy-start | bytes 1769476
  56.7 250.9 %all-gather.8.cloned.1.call-start = ((), (), s32[]{:S(2)}) async-start(), calls=%async_computation.7 | async-start | bytes 2949120 | tf_op jit(solution)/shard_map/all_gather | solution.py:46
  58.4 299.9 %reduce-scatter.2.cloned.1.call-start = ((), (), s32[]{:S(2)}) async-start(), calls=%async_computation.8 | async-start | bytes 2949120 | tf_op jit(solution)/shard_map/reduce_scatter | solution.py:55
Sparse Core Ops, SparseCore 0:
  33.3 124.9 all-gather.3
  160.5 122.6 all-gather.5
  285.3 22.2 all-gather.7
  325.5 32.8 reduce-scatter.1
where the time goes:
time: 365 us
  waiting for transfers between devices  265 us (73%)
  blocking collectives  43.9 us (12%)
  local copies, waits for them, and re-layouts  22.3 us (6%)
  matrix products  17.7 us (5%)
  between operations  13.8 us (4%)
    all_gather x1, waiting for transfers between devices, body(): lax.all_gather(moved[1], 'fs', axis=0, tiled=True)  116 us
    all_gather x1, waiting for transfers between devices, body(): lax.all_gather(moved[0], 'fs', axis=0, tiled=True)  99.9 us
    reduce_scatter x1, waiting for transfers between devices, body(): lax.psum_scatter(lax.optimization_barrier(partial_value.astype(jnp.bfloat...  33 us
    all_to_all x1, blocking collectives, body(): lax.all_to_all(lax.all_to_all(up_local, 'tp', split_axis=1, concat_axis=0...  18 us
    dot_general x1, matrix products, body(): lax.dot_general(hidden, sampler_down, (((1,), (1,)), ((), ())), preferred...  17.7 us
    transpose x2, local copies, waits for them, and re-layouts, regroup(): shaped.transpose(1, 0, 2, 3)  17.1 us
    all_to_all x1, blocking collectives, body(): lax.all_to_all(lax.all_to_all(down_local, 'tp', split_axis=1, concat_axis...  16.7 us
    all_gather x1, waiting for transfers between devices, body(): lax.all_gather(normed, ('gr', 'tp'), axis=0, tiled=True)  15.8 us
  transfers between devices with their start and end apart: 4, of which 4 were waited for; matrix products, arithmetic and copies ran while one was open for 6% of the time, Pallas kernels for 0%

commit v1 on v0

v1 whole, which is shorter than its diff:
```python
import functools

import jax
import jax.numpy as jnp
from jax import lax
from jax.experimental import pallas as pl
from jax.experimental.pallas import tpu as pltpu
from jax.sharding import PartitionSpec as P

MESH = pl.DeviceIdType.MESH
CHUNK = 32
TILE = 256
PAIR_FIRST = (1, 2)


def kernel(G, F, T, tok_in, up_in, down_in, up_out, down_out, out_ref,
           full, nrm, hid, stage, part,
           recv, sendl, sendr, sendy, send0, tok_recv, tok_send,
           part_recv, part_send, local_sem):
    gr, f, tp = lax.axis_index("gr"), lax.axis_index("fs"), lax.axis_index("tp")
    A = F // 2
    a, y = f // 2, f % 2
    mate = a * 2 + 1 - y
    R = up_in.shape[0]
    D = full.shape[1]
    W = full.shape[2]
    tok = tok_in.shape[0]
    CH = min(CHUNK, R)
    C = R // CH
    NQ = G * C
    K = G * T
    k = gr * T + tp
    weights = (up_in, down_in)

    def at_k(kk):
        return (kk // T, f, kk % T)

    barrier = pltpu.get_barrier_semaphore()
    for d in range(1, K):
        pl.semaphore_signal(barrier, inc=1, device_id=at_k((k + d) % K), device_id_type=MESH)
    pl.semaphore_signal(barrier, inc=1, device_id=(gr, mate, tp), device_id_type=MESH)

    for shift in (1, A - 1):
        near = lax.rem(a + shift, A) * 2 + y
        pl.semaphore_signal(barrier, inc=1, device_id=(gr, near, tp), device_id_type=MESH)
    pl.semaphore_wait(barrier, K + 2)

    def rows_of(origin, g, c):
        return pl.ds(pl.multiple_of(g * (F * R) + origin * R + c * CH, CH), CH)

    def hand(m, b, c, wait):
        kk = tp * G + b
        dg = kk // T
        q = ((gr - dg + G) % G) * C + c
        src = weights[m].at[pl.ds(c * CH, CH), pl.ds(b * W, W)]
        dst = full.at[m, rows_of(f, gr, c)]

        @pl.when(kk == k)
        def _():
            if not wait:
                pltpu.make_async_copy(src, dst, recv.at[m, f, q]).start()

        @pl.when(kk != k)
        def _():
            copy = pltpu.make_async_remote_copy(
                src_ref=src, dst_ref=dst, send_sem=send0.at[m, b, c], recv_sem=recv.at[m, f, q],
                device_id=at_k(kk), device_id_type=MESH)
            if wait:
                copy.wait_send()
            else:
                copy.start()

    def tokens(wait):
        own = nrm.at[pl.ds(pl.multiple_of(k * tok, 16), tok)]
        if not wait:
            pltpu.make_async_copy(tok_in, own, local_sem.at[0]).start()
        for d in range(1, K):
            copy = pltpu.make_async_remote_copy(
                src_ref=tok_in, dst_ref=own, send_sem=tok_send.at[d - 1], recv_sem=tok_recv.at[d - 1],
                device_id=at_k((k + d) % K), device_id_type=MESH)
            if wait:
                copy.wait_send()
            else:
                copy.start()

    for m in range(2):
        for c in range(C):
            for b in range(G):
                hand(m, b, c, False)
        if m == 0:
            tokens(False)

    def chunk(m, origin, q):
        return full.at[m, rows_of(origin, (gr + q // C) % G, q % C)]

    def send(m, origin, q, sems, target, wait):
        ref = chunk(m, origin, q)
        copy = pltpu.make_async_remote_copy(
            src_ref=ref, dst_ref=ref, send_sem=sems.at[m, origin, q], recv_sem=recv.at[m, origin, q],
            device_id=(gr, target, tp), device_id_type=MESH)
        if wait:
            copy.wait_send()
        else:
            copy.start()

    def arrived(m, origin, q):
        ref = chunk(m, origin, q)
        pltpu.make_async_copy(ref, ref, recv.at[m, origin, q]).wait()

    def left(m, origin, q, wait):
        @pl.when(a > 0)
        def _():
            send(m, origin, q, sendl, f - 2, wait)

    def right(m, origin, q, wait):
        @pl.when(a < A - 1)
        def _():
            send(m, origin, q, sendr, f + 2, wait)

    def loop(low, high, step):
        def go(i, carry):
            step(i)
            return carry
        if high > low:
            lax.fori_loop(low, high, go, 0)

    def own(m, wait=False):
        def step(q):
            if not wait:
                arrived(m, f, q)
            left(m, f, q, wait)
            right(m, f, q, wait)
            send(m, f, q, sendy, mate, wait)
        loop(0, NQ, step)

    def mated(m, wait=False):
        def step(q):
            if not wait:
                arrived(m, mate, q)
            left(m, mate, q, wait)
            right(m, mate, q, wait)
        loop(0, PAIR_FIRST[m], step)

    def line(m, s, wait=False):
        below, above = a - 1 - s, a + 1 + s

        def pass_on(origin_a, side, q, onward, across):
            origin = origin_a * 2 + side
            if not wait:
                arrived(m, origin, q)
            onward(m, origin, q, wait)
            if across:
                send(m, origin, q, sendy, mate, wait)

        def both(side, across):
            def step(q):
                @pl.when(below >= 0)
                def _():
                    pass_on(below, side, q, right, across)

                @pl.when(above < A)
                def _():
                    pass_on(above, side, q, left, across)
            return step

        pf = PAIR_FIRST[m]
        loop(0, pf, both(y, False))
        loop(pf, NQ, both(y, True))
        loop(0, pf, both(1 - y, False))

    def settle(m, origin_a):
        loop(PAIR_FIRST[m], NQ, lambda q: arrived(m, origin_a * 2 + 1 - y, q))

    own(0)
    mated(0)
    loop(0, A - 2, lambda s: line(0, s))
    own(1)
    line(0, A - 2)
    mated(1)
    line(1, 0)

    loop(0, A, lambda i: settle(0, i))
    up_copy = pltpu.make_async_copy(full.at[0], up_out, local_sem.at[1])
    up_copy.start()
    pltpu.make_async_copy(tok_in, nrm.at[pl.ds(pl.multiple_of(k * tok, 16), tok)], local_sem.at[0]).wait()
    for d in range(1, K):
        there = nrm.at[pl.ds(pl.multiple_of(((k - d + K) % K) * tok, 16), tok)]
        pltpu.make_async_copy(there, there, tok_recv.at[d - 1]).wait()

    tile = min(TILE, W)

    def lift(j):
        columns = pl.ds(pl.multiple_of(j * tile, tile), tile)
        lifted = jnp.maximum(jnp.dot(nrm[...], full[0, :, columns], preferred_element_type=jnp.float32), 0.0)
        hid[:, columns] = (lifted * lifted).astype(jnp.bfloat16)
    loop(0, W // tile, lift)

    def part_copy(d, block):
        target = (k + d) % K
        return pltpu.make_async_remote_copy(
            src_ref=stage.at[block, pl.ds(pl.multiple_of(target * tok, 16), tok)],
            dst_ref=part.at[d - 1, block],
            send_sem=part_send.at[d - 1, block], recv_sem=part_recv.at[d - 1, block],
            device_id=at_k(target), device_id_type=MESH)

    def lower(origin_a):
        settle(1, origin_a)

        def group(g):
            block = origin_a * G + g
            rows = pl.ds(pl.multiple_of(g * (F * R) + origin_a * (2 * R), 2 * R), 2 * R)
            pltpu.make_async_copy(full.at[1, rows], down_out.at[rows], local_sem.at[2 + block]).start()
            value = lax.dot_general(hid[...], full[1, rows, :], (((1,), (1,)), ((), ())),
                                    preferred_element_type=jnp.float32)
            stage[block] = value.astype(jnp.bfloat16)
            for d in range(1, K):
                part_copy(d, block).start()
        loop(0, G, group)

    def lower_ring(s):
        @pl.when(a - 1 - s >= 0)
        def _():
            lower(a - 1 - s)

        @pl.when(a + 1 + s < A)
        def _():
            lower(a + 1 + s)

    lower(a)

    def tail(s):
        line(1, s)
        lower_ring(s - 1)
    loop(1, A - 1, tail)
    lower_ring(A - 2)

    mine = pl.ds(pl.multiple_of(k * tok, 16), tok)
    for block in range(A * G):
        total = stage[block, mine].astype(jnp.float32)
        for d in range(1, K):
            there = part.at[d - 1, block]
            pltpu.make_async_copy(there, there, part_recv.at[d - 1, block]).wait()
            total += part[d - 1, block].astype(jnp.float32)
        begin = (block % G) * (F * R) + (block // G) * (2 * R)
        out_ref[:, begin:begin + 2 * R] = total.astype(jnp.bfloat16)

    up_copy.wait()

    def drain(block):
        rows = pl.ds(0, 2 * R)
        pltpu.make_async_copy(full.at[1, rows], down_out.at[rows], local_sem.at[2 + block]).wait()
        for d in range(1, K):
            part_copy(d, block).wait_send()
    loop(0, A * G, drain)
    tokens(True)
    for m in range(2):
        for c in range(C):
            for b in range(G):
                hand(m, b, c, True)
        own(m, True)
        mated(m, True)
        loop(0, A - 1, lambda s: line(m, s, True))


def body(G, F, T, prompt_tokens, up_master, down_master, norm_gain):
    up_local = (norm_gain[:, None] * up_master).astype(jnp.bfloat16)
    down_local = down_master.astype(jnp.bfloat16)
    values = prompt_tokens.astype(jnp.float32)
    center = jnp.mean(values, axis=-1, keepdims=True)
    variance = jnp.mean(jnp.square(values - center), axis=-1, keepdims=True)
    normed = ((values - center) * lax.rsqrt(variance + 1e-05)).astype(jnp.bfloat16)
    R, width = up_local.shape
    tok = normed.shape[0]
    D, W = R * G * F, width // G
    A, K = F // 2, G * T
    C = R // min(CHUNK, R)
    NQ = G * C
    bf16 = jnp.bfloat16
    any_space = pl.BlockSpec(memory_space=pl.ANY)
    dma = pltpu.SemaphoreType.DMA
    return pl.pallas_call(
        functools.partial(kernel, G, F, T),
        name="handoff",
        out_shape=(
            jax.ShapeDtypeStruct((D, W), bf16),
            jax.ShapeDtypeStruct((D, W), bf16),
            jax.ShapeDtypeStruct((tok, D), bf16),
        ),
        in_specs=[any_space] * 3,
        out_specs=(any_space, any_space, pl.BlockSpec(memory_space=pltpu.VMEM)),
        scratch_shapes=[
            pltpu.VMEM((2, D, W), bf16),
            pltpu.VMEM((K * tok, D), bf16),
            pltpu.VMEM((K * tok, W), bf16),
            pltpu.VMEM((A * G, K * tok, 2 * R), bf16),
            pltpu.VMEM((K - 1, A * G, tok, 2 * R), bf16),
            dma((2, F, NQ)), dma((2, F, NQ)), dma((2, F, NQ)), dma((2, F, NQ)),
            dma((2, G, C)), dma((K - 1,)), dma((K - 1,)),
            dma((K - 1, A * G)), dma((K - 1, A * G)), dma((2 + A * G,)),
        ],
        compiler_params=pltpu.CompilerParams(
            collective_id=0, has_side_effects=True, vmem_limit_bytes=56 * 1024 * 1024),
    )(normed, up_local, down_local)


def solution(mesh):
    placed = (
        P(("gr", "fs", "tp"), None),
        P(("gr", "fs"), "tp"),
        P(("gr", "fs"), "tp"),
        P(("gr", "fs")),
    )
    return jax.shard_map(
        functools.partial(body, mesh.shape["gr"], mesh.shape["fs"], mesh.shape["tp"]),
        mesh=mesh,
        in_specs=placed,
        out_specs=(P(None, ("gr", "tp")), P(None, ("gr", "tp")), P(("gr", "fs", "tp"), None)),
        check_vma=False,
    )
```

time: 365 us -> 215 us (0.59)
  waiting for transfers between devices: 265 us -> 0 us
  Pallas kernels: 0 us -> 188 us
  blocking collectives: 43.9 us -> 0 us
  matrix products: 17.7 us -> 0 us
  between operations: 13.8 us -> 0.66 us
  other arithmetic: 1.78 us -> 7.87 us
  local copies, waits for them, and re-layouts: 22.3 us -> 17.8 us
    all_gather x3 -> x0, waiting for transfers between devices: 232 us -> none  [the longest x1 116 us: body(): lax.all_gather(moved[1], 'fs', axis=0, tiled=True)]
    pallas_call x0 -> x1, Pallas kernels: none -> 188 us  [body(): pl.pallas_call(functools.partial(kernel, G, F, T), name='handoff', out_sh...]
    all_to_all x4 -> x0, blocking collectives: 43.9 us -> none  [the longest x1 18 us: body(): lax.all_to_all(lax.all_to_all(up_local, 'tp', split_axis=1, concat_axis=0...]
    reduce_scatter x1 -> x0, waiting for transfers between devices: 33 us -> none  [body(): lax.psum_scatter(lax.optimization_barrier(partial_value.astype(jnp.bfloat...]
    dot_general x1 -> x0, matrix products: 17.7 us -> none  [body(): lax.dot_general(hidden, sampler_down, (((1,), (1,)), ((), ())), preferred...]
    transpose x2 -> x0, local copies, waits for them, and re-layouts: 17.1 us -> none  [regroup(): shaped.transpose(1, 0, 2, 3)]
    unnamed x8 -> x11, local copies, waits for them, and re-layouts: 2.66 us -> 17.8 us
  transfers between devices with their start and end apart: 4 -> 0, of which waited for: 4 -> 0; matrix products, arithmetic and copies ran while one was open for 6% -> 0% of each run, Pallas kernels for 0% -> 0%
where the time goes in v1:
time: 215 us; the launch traced here: 214 us
  Pallas kernels  188 us (87%)
  local copies, waits for them, and re-layouts  17.8 us (8%)
  other arithmetic  7.87 us (4%)
    pallas_call x1, Pallas kernels, body(): pl.pallas_call(functools.partial(kernel, G, F, T), name='handoff', out_sh...  188 us
    unnamed x11, local copies, waits for them, and re-layouts  17.8 us

profile of v1, /device:TPU:0, one launch (start us, length us, event | category | flops | bytes accessed | tf_op | source)
XLA Modules:
  0.0 214.2 jit_solution(5363656045602658737)
XLA Ops:
  0.6 0.0 copy-start
  0.6 0.0 copy-start.3
  0.7 1.3 convert_reduce_fusion
  1.9 1.4 fusion.2
  3.3 0.0 copy-done
  3.3 1.2 fusion.3.tok_in
  4.5 0.0 copy-done.3
  4.5 0.0 copy-start.1
  4.5 2.9 %multiply_convert_fusion.up_in = bf16[128,4096]{1,0:T(8,128)(2,1)} fusion(f32[128,4096]{1,0:T(8,128)} %param.5, f32[128]{0:T(128)S(1)} %copy-done.3), kind=kLoop, calls=%fused_computation | loop fusion | flops 1048576 | bytes 3146240 | tf_op jit(solution)/shard_map/convert_element_type | solution.py:266
  7.4 0.0 copy-done.1
  7.4 1.1 convert_element_type.15.down_in
  8.5 187.9 %handoff.1 = (bf16[2048,2048]{1,0:T(8,128)(2,1)}, bf16[2048,2048]{1,0:T(8,128)(2,1)}, bf16[144,2048]{1,0:T(8,128)(2,1)}) custom-call(bf16[144,2048]{1,0:T(8,128)(2,1)} %fusion.3.tok_in, bf16[128,4096]{1,0:T(8,128)(2,1)} %multiply_convert_fusion.up_in, bf16[128,4096]{1,0:T(8,128)(2,1)} %convert_element_type.15.down_in), custom_call_target="tpu_custom_call" | custom-call | tf_op jit(solution)/shard_map/handoff/pallas_call | solution.py:281
  196.4 8.4 %copy.10 = bf16[2048,2048]{1,0:T(8,128)(2,1)} copy(bf16[2048,2048]{1,0:T(8,128)(2,1)} %get-tuple-element.6) | data formatting | bytes 16777216
  204.9 0.0 copy-start.2
  204.9 8.5 %copy.11 = bf16[2048,2048]{1,0:T(8,128)(2,1)} copy(bf16[2048,2048]{1,0:T(8,128)(2,1)} %get-tuple-element.7) | data formatting | bytes 16777216
  213.4 0.0 copy-done.2
  213.4 0.8 copy.12
  (2 shorter events, 0.0 us)
Async XLA Ops:
  0.6 2.7 %copy-start = (bf16[144,2048]{1,0:T(8,128)(2,1)S(1)}, bf16[144,2048]{1,0:T(8,128)(2,1)}, u32[]{:S(2)}) copy-start(bf16[144,2048]{1,0:T(8,128)(2,1)} %param.4) | copy-start | bytes 1769476
  0.6 3.9 %copy-start.3 = (f32[128]{0:T(128)S(1)}, f32[128]{0:T(128)}, u32[]{:S(2)}) copy-start(f32[128]{0:T(128)} %param.7) | copy-start | bytes 1540
  4.5 2.9 %copy-start.1 = (f32[128,4096]{1,0:T(8,128)S(1)}, f32[128,4096]{1,0:T(8,128)}, u32[]{:S(2)}) copy-start(f32[128,4096]{1,0:T(8,128)} %param.6) | copy-start | bytes 6291460
  204.9 8.5 %copy-start.2 = (bf16[144,2048]{1,0:T(8,128)(2,1)S(1)}, bf16[144,2048]{1,0:T(8,128)(2,1)}, u32[]{:S(2)}) copy-start(bf16[144,2048]{1,0:T(8,128)(2,1)} %get-tuple-element.8) | copy-start | bytes 1769476

commit v2 on v1

v2 whole, which is shorter than its diff:
```python
import functools

import jax
import jax.numpy as jnp
from jax import lax
from jax.experimental import pallas as pl
from jax.experimental.pallas import tpu as pltpu
from jax.sharding import PartitionSpec as P

MESH = pl.DeviceIdType.MESH
CHUNK = 32
TILE = 256
PAIR_FIRST = (1, 2)


def kernel(G, F, T, tok_in, gain_in, up_in, down_in, up_full, down_full, out_ref,
           wide, narrow, raw, nrm, hid, stage, part,
           recv, sendl, sendr, sendy, send0, tok_recv, tok_send,
           part_recv, part_send, local_sem, load_sem):
    gr, f, tp = lax.axis_index("gr"), lax.axis_index("fs"), lax.axis_index("tp")
    full = (up_full, down_full)
    A = F // 2
    a, y = f // 2, f % 2
    mate = a * 2 + 1 - y
    R = up_in.shape[0]
    D, W = up_full.shape
    tok = tok_in.shape[0]
    CH = min(CHUNK, R)
    C = R // CH
    NQ = G * C
    K = G * T
    k = gr * T + tp
    weights = (up_in, down_in)

    def at_k(kk):
        return (kk // T, f, kk % T)

    def load(m, c):
        rows = pl.ds(c * CH, CH)
        return pltpu.make_async_copy(weights[m].at[rows], wide.at[m, rows], load_sem.at[m, c])

    token_load = pltpu.make_async_copy(tok_in, raw, local_sem.at[0])
    for c in range(C):
        load(0, c).start()
    token_load.start()
    for c in range(C):
        load(1, c).start()

    barrier = pltpu.get_barrier_semaphore()
    for d in range(1, K):
        pl.semaphore_signal(barrier, inc=1, device_id=at_k((k + d) % K), device_id_type=MESH)
    pl.semaphore_signal(barrier, inc=1, device_id=(gr, mate, tp), device_id_type=MESH)

    for shift in (1, A - 1):
        near = lax.rem(a + shift, A) * 2 + y
        pl.semaphore_signal(barrier, inc=1, device_id=(gr, near, tp), device_id_type=MESH)
    pl.semaphore_wait(barrier, K + 2)

    def rows_of(origin, g, c):
        return pl.ds(pl.multiple_of(g * (F * R) + origin * R + c * CH, CH), CH)

    home = k // G == tp

    def cast(m, c):
        rows = pl.ds(c * CH, CH)
        load(m, c).wait()
        value = wide[m, rows, :]
        if m == 0:
            value = value * column[c * CH:(c + 1) * CH]
        value = value.astype(jnp.bfloat16)
        narrow[m, rows, :] = value
        for b in range(G):
            @pl.when(tp * G + b == k)
            def _():
                full[m][rows_of(f, gr, c), :] = value[:, b * W:(b + 1) * W]

    def hand(m, b, c, wait):
        kk = tp * G + b
        q = ((gr - kk // T + G) % G) * C + c

        @pl.when(kk != k)
        def _():
            copy = pltpu.make_async_remote_copy(
                src_ref=narrow.at[m, pl.ds(c * CH, CH), pl.ds(b * W, W)],
                dst_ref=full[m].at[rows_of(f, gr, c)],
                send_sem=send0.at[m, b, c], recv_sem=recv.at[m, f, q],
                device_id=at_k(kk), device_id_type=MESH)
            if wait:
                copy.wait_send()
            else:
                copy.start()

    mine = pl.ds(pl.multiple_of(k * tok, 16), tok)

    def tokens(wait):
        for d in range(1, K):
            copy = pltpu.make_async_remote_copy(
                src_ref=nrm.at[mine], dst_ref=nrm.at[mine],
                send_sem=tok_send.at[d - 1], recv_sem=tok_recv.at[d - 1],
                device_id=at_k((k + d) % K), device_id_type=MESH)
            if wait:
                copy.wait_send()
            else:
                copy.start()

    def normalize(i, carry):
        values = raw[pl.ds(pl.multiple_of(i * 16, 16), 16), :].astype(jnp.float32)
        center = jnp.mean(values, axis=-1, keepdims=True)
        moved = values - center
        spread = jnp.mean(jnp.square(moved), axis=-1, keepdims=True)
        nrm[pl.ds(pl.multiple_of(k * tok + i * 16, 16), 16), :] = (
            moved * lax.rsqrt(spread + 1e-05)).astype(jnp.bfloat16)
        return carry

    rowed = lax.broadcasted_iota(jnp.int32, (R, R), 0) == lax.broadcasted_iota(jnp.int32, (R, R), 1)
    column = jnp.sum(jnp.where(rowed, gain_in[...], 0.0), axis=1, keepdims=True)

    cast(0, 0)
    for c in range(C):
        if c + 1 < C:
            cast(0, c + 1)
        else:
            cast(1, 0)
        for b in range(G):
            hand(0, b, c, False)

    def chunk(m, origin, q):
        return full[m].at[rows_of(origin, (gr + q // C) % G, q % C)]

    def send(m, origin, q, sems, target, wait):
        ref = chunk(m, origin, q)
        copy = pltpu.make_async_remote_copy(
            src_ref=ref, dst_ref=ref, send_sem=sems.at[m, origin, q], recv_sem=recv.at[m, origin, q],
            device_id=(gr, target, tp), device_id_type=MESH)
        if wait:
            copy.wait_send()
        else:
            copy.start()

    def arrived(m, origin, q):
        ref = chunk(m, origin, q)
        pltpu.make_async_copy(ref, ref, recv.at[m, origin, q]).wait()

    def left(m, origin, q, wait):
        @pl.when(a > 0)
        def _():
            send(m, origin, q, sendl, f - 2, wait)

    def right(m, origin, q, wait):
        @pl.when(a < A - 1)
        def _():
            send(m, origin, q, sendr, f + 2, wait)

    def loop(low, high, step):
        def go(i, carry):
            step(i)
            return carry
        if high > low:
            lax.fori_loop(low, high, go, 0)

    def own(m, wait=False):
        def step(q):
            if not wait:
                @pl.when(jnp.logical_or(q >= C, jnp.logical_not(home)))
                def _():
                    arrived(m, f, q)
            left(m, f, q, wait)
            right(m, f, q, wait)
            send(m, f, q, sendy, mate, wait)
        loop(0, NQ, step)

    def mated(m, wait=False):
        def step(q):
            if not wait:
                arrived(m, mate, q)
            left(m, mate, q, wait)
            right(m, mate, q, wait)
        loop(0, PAIR_FIRST[m], step)

    def line(m, s, wait=False, between=None):
        below, above = a - 1 - s, a + 1 + s

        def pass_on(origin_a, side, q, onward, across):
            origin = origin_a * 2 + side
            if not wait:
                arrived(m, origin, q)
            onward(m, origin, q, wait)
            if across:
                send(m, origin, q, sendy, mate, wait)

        def both(side, across):
            def step(q):
                @pl.when(below >= 0)
                def _():
                    pass_on(below, side, q, right, across)

                @pl.when(above < A)
                def _():
                    pass_on(above, side, q, left, across)
            return step

        pf = PAIR_FIRST[m]
        loop(0, pf, both(y, False))
        half = NQ // 2 + 1 if between is not None else NQ
        loop(pf, half, both(y, True))
        if between is not None:
            between()
        loop(half, NQ, both(y, True))
        loop(0, pf, both(1 - y, False))

    def settle(m, origin_a, gi):
        low = jnp.maximum(PAIR_FIRST[m], gi * C)

        def go(q, carry):
            arrived(m, origin_a * 2 + 1 - y, q)
            return carry
        lax.fori_loop(low, (gi + 1) * C, go, 0)

    def settle_all(i):
        for gi in range(G):
            settle(0, i, gi)

    own(0)
    token_load.wait()
    lax.fori_loop(0, tok // 16, normalize, 0)
    for c in range(C):
        if c + 1 < C:
            cast(1, c + 1)
        for b in range(G):
            hand(1, b, c, False)
    tokens(False)
    mated(0)
    loop(0, A - 2, lambda s: line(0, s))
    own(1)
    line(0, A - 2)
    mated(1)
    line(1, 0)

    loop(0, A, settle_all)
    for d in range(1, K):
        there = nrm.at[pl.ds(pl.multiple_of(((k - d + K) % K) * tok, 16), tok)]
        pltpu.make_async_copy(there, there, tok_recv.at[d - 1]).wait()

    tile = min(TILE, W)

    def lift(j):
        columns = pl.ds(pl.multiple_of(j * tile, tile), tile)
        lifted = jnp.maximum(jnp.dot(nrm[...], up_full[:, columns], preferred_element_type=jnp.float32), 0.0)
        hid[:, columns] = (lifted * lifted).astype(jnp.bfloat16)
    loop(0, W // tile, lift)

    def part_copy(d, block):
        target = (k + d) % K
        return pltpu.make_async_remote_copy(
            src_ref=stage.at[block, pl.ds(pl.multiple_of(target * tok, 16), tok)],
            dst_ref=part.at[d - 1, block],
            send_sem=part_send.at[d - 1, block], recv_sem=part_recv.at[d - 1, block],
            device_id=at_k(target), device_id_type=MESH)

    def lower(origin_a):
        def group(gi):
            settle(1, origin_a, gi)
            g = (gr + gi) % G
            block = origin_a * G + g
            rows = pl.ds(pl.multiple_of(g * (F * R) + origin_a * (2 * R), 2 * R), 2 * R)
            value = lax.dot_general(hid[...], down_full[rows, :], (((1,), (1,)), ((), ())),
                                    preferred_element_type=jnp.float32)
            stage[block] = value.astype(jnp.bfloat16)
            for d in range(1, K):
                part_copy(d, block).start()
        loop(0, G, group)

    def lower_ring(s):
        @pl.when(a - 1 - s >= 0)
        def _():
            lower(a - 1 - s)

        @pl.when(a + 1 + s < A)
        def _():
            lower(a + 1 + s)

    lower(a)
    loop(1, A - 1, lambda s: line(1, s, between=lambda: lower_ring(s - 1)))
    lower_ring(A - 2)

    for block in range(A * G):
        total = stage[block, mine].astype(jnp.float32)
        for d in range(1, K):
            there = part.at[d - 1, block]
            pltpu.make_async_copy(there, there, part_recv.at[d - 1, block]).wait()
            total += part[d - 1, block].astype(jnp.float32)
        begin = (block % G) * (F * R) + (block // G) * (2 * R)
        out_ref[:, begin:begin + 2 * R] = total.astype(jnp.bfloat16)

    def drain(block):
        for d in range(1, K):
            part_copy(d, block).wait_send()
    loop(0, A * G, drain)
    tokens(True)
    for m in range(2):
        for c in range(C):
            for b in range(G):
                hand(m, b, c, True)
        own(m, True)
        mated(m, True)
        loop(0, A - 1, lambda s: line(m, s, True))


def body(G, F, T, prompt_tokens, up_master, down_master, norm_gain):
    R, width = up_master.shape
    tok = prompt_tokens.shape[0]
    D, W = R * G * F, width // G
    A, K = F // 2, G * T
    C = R // min(CHUNK, R)
    NQ = G * C
    bf16 = jnp.bfloat16
    any_space = pl.BlockSpec(memory_space=pl.ANY)
    vmem_space = pl.BlockSpec(memory_space=pltpu.VMEM)
    dma = pltpu.SemaphoreType.DMA
    return pl.pallas_call(
        functools.partial(kernel, G, F, T),
        name="handoff",
        out_shape=(
            pltpu.MemorySpace.VMEM((D, W), bf16),
            pltpu.MemorySpace.VMEM((D, W), bf16),
            jax.ShapeDtypeStruct((tok, D), bf16),
        ),
        in_specs=[any_space, vmem_space, any_space, any_space],
        out_specs=(vmem_space,) * 3,
        scratch_shapes=[
            pltpu.VMEM((2, R, width), jnp.float32),
            pltpu.VMEM((2, R, width), bf16),
            pltpu.VMEM((tok, D), bf16),
            pltpu.VMEM((K * tok, D), bf16),
            pltpu.VMEM((K * tok, W), bf16),
            pltpu.VMEM((A * G, K * tok, 2 * R), bf16),
            pltpu.VMEM((K - 1, A * G, tok, 2 * R), bf16),
            dma((2, F, NQ)), dma((2, F, NQ)), dma((2, F, NQ)), dma((2, F, NQ)),
            dma((2, G, C)), dma((K - 1,)), dma((K - 1,)),
            dma((K - 1, A * G)), dma((K - 1, A * G)), dma((1,)), dma((2, C)),
        ],
        compiler_params=pltpu.CompilerParams(
            collective_id=0, has_side_effects=True, vmem_limit_bytes=43 * 1024 * 1024),
    )(prompt_tokens, norm_gain.reshape(1, R), up_master, down_master)


def solution(mesh):
    placed = (
        P(("gr", "fs", "tp"), None),
        P(("gr", "fs"), "tp"),
        P(("gr", "fs"), "tp"),
        P(("gr", "fs")),
    )
    return jax.shard_map(
        functools.partial(body, mesh.shape["gr"], mesh.shape["fs"], mesh.shape["tp"]),
        mesh=mesh,
        in_specs=placed,
        out_specs=(P(None, ("gr", "tp")), P(None, ("gr", "tp")), P(("gr", "fs", "tp"), None)),
        check_vma=False,
    )
```

time: 215 us -> 190 us (0.88)
  local copies, waits for them, and re-layouts: 17.8 us -> 7.61 us
  other arithmetic: 7.87 us -> 0 us
  Pallas kernels: 188 us -> 182 us
    unnamed x11 -> x5, local copies, waits for them, and re-layouts: 17.8 us -> 7.61 us
    pallas_call x1, Pallas kernels: 188 us -> 182 us  [body(): pl.pallas_call(functools.partial(kernel, G, F, T), name='handoff', out_sh...]
    convert_element_type x3 -> x0, other arithmetic: 5.2 us -> none  [the longest x1 2.93 us: body(): up_local = (norm_gain[:, None] * up_master).astype(jnp.bfloat16)]
    reduce_sum x2 -> x0, other arithmetic: 2.66 us -> none  [the longest x1 1.37 us: body(): variance = jnp.mean(jnp.square(values - center), axis=-1, keepdims=True)]
where the time goes in v2:
time: 190 us
  Pallas kernels  182 us (96%)
  local copies, waits for them, and re-layouts  7.61 us (4%)
    pallas_call x1, Pallas kernels, body(): pl.pallas_call(functools.partial(kernel, G, F, T), name='handoff', out_sh...  182 us
    unnamed x5, local copies, waits for them, and re-layouts  7.61 us

profile of v2, /device:TPU:0, one launch (start us, length us, event | category | flops | bytes accessed | tf_op | source)
XLA Modules:
  0.0 190.1 jit_solution(15605375373543978521)
XLA Ops:
  0.6 181.8 %handoff.1 = (bf16[2048,2048]{1,0:T(8,128)(2,1)S(1)}, bf16[2048,2048]{1,0:T(8,128)(2,1)S(1)}, bf16[144,2048]{1,0:T(8,128)(2,1)}) custom-call(bf16[144,2048]{1,0:T(8,128)(2,1)} %tok_in.1, f32[1,128]{1,0:T(1,128)} %bitcast.1, f32[128,4096]{1,0:T(8,128)} %up_in.1, f32[128,4096]{1,0:T(8,128)} %down_in.1), custom_call_target="tpu_custom_call" | custom-call | tf_op jit(solution)/shard_map/handoff/pallas_call | solution.py:320
  182.5 3.4 %copy.10 = bf16[2048,2048]{1,0:T(8,128)(2,1)} copy(bf16[2048,2048]{1,0:T(8,128)(2,1)S(1)} %get-tuple-element.3) | data formatting | bytes 16777216
  185.9 0.0 copy-start
  185.9 3.4 %copy.11 = bf16[2048,2048]{1,0:T(8,128)(2,1)} copy(bf16[2048,2048]{1,0:T(8,128)(2,1)S(1)} %get-tuple-element.4) | data formatting | bytes 16777216
  189.2 0.0 copy-done
  189.3 0.8 copy.12
Async XLA Ops:
  185.9 3.4 %copy-start = (bf16[144,2048]{1,0:T(8,128)(2,1)S(1)}, bf16[144,2048]{1,0:T(8,128)(2,1)}, u32[]{:S(2)}) copy-start(bf16[144,2048]{1,0:T(8,128)(2,1)} %get-tuple-element.11) | copy-start | bytes 1769476

commit v3 on v2

--- a/solution.py
+++ b/solution.py
@@ -8,13 +8,13 @@
 from jax.sharding import PartitionSpec as P
 
 MESH = pl.DeviceIdType.MESH
-CHUNK = 32
+CHUNK = 16
 TILE = 256
-PAIR_FIRST = (1, 2)
-
-
-def kernel(G, F, T, tok_in, gain_in, up_in, down_in, up_full, down_full, out_ref,
-           wide, narrow, raw, nrm, hid, stage, part,
+SPLIT = 4
+
+
+def kernel(G, F, T, tok_in, gain_in, up_in, down_in, up_full, down_full, part,
+           wide, narrow, raw, nrm, hid, stage,
            recv, sendl, sendr, sendy, send0, tok_recv, tok_send,
            part_recv, part_send, local_sem, load_sem):
     gr, f, tp = lax.axis_index("gr"), lax.axis_index("fs"), lax.axis_index("tp")
@@ -28,6 +28,7 @@
     CH = min(CHUNK, R)
     C = R // CH
     NQ = G * C
+    PAIR_FIRST = (NQ * 5 // 32, (NQ * 5 + 31) // 32)
     K = G * T
     k = gr * T + tp
     weights = (up_in, down_in)
@@ -167,7 +168,12 @@
             left(m, f, q, wait)
             right(m, f, q, wait)
             send(m, f, q, sendy, mate, wait)
-        loop(0, NQ, step)
+        if m == 0:
+            loop(0, NQ, step)
+        else:
+            loop(0, PAIR_FIRST[m], step)
+            loop(C, NQ, step)
+            loop(PAIR_FIRST[m], C, step)
 
     def mated(m, wait=False):
         def step(q):
@@ -177,7 +183,7 @@
             right(m, mate, q, wait)
         loop(0, PAIR_FIRST[m], step)
 
-    def line(m, s, wait=False, between=None):
+    def line(m, s, wait=False, between=None, eager=None):
         below, above = a - 1 - s, a + 1 + s
 
         def pass_on(origin_a, side, q, onward, across):
@@ -201,11 +207,15 @@
 
         pf = PAIR_FIRST[m]
         loop(0, pf, both(y, False))
-        half = NQ // 2 + 1 if between is not None else NQ
-        loop(pf, half, both(y, True))
-        if between is not None:
-            between()
-        loop(half, NQ, both(y, True))
+        if m == 0:
+            loop(pf, NQ, both(y, True))
+        else:
+            loop(C, NQ, both(y, True))
+            if between is not None:
+                between()
+            loop(pf, C, both(y, True))
+        if eager is not None:
+            eager()
         loop(0, pf, both(1 - y, False))
 
     def settle(m, origin_a, gi):
@@ -257,40 +267,37 @@
             send_sem=part_send.at[d - 1, block], recv_sem=part_recv.at[d - 1, block],
             device_id=at_k(target), device_id_type=MESH)
 
-    def lower(origin_a):
-        def group(gi):
-            settle(1, origin_a, gi)
-            g = (gr + gi) % G
-            block = origin_a * G + g
-            rows = pl.ds(pl.multiple_of(g * (F * R) + origin_a * (2 * R), 2 * R), 2 * R)
-            value = lax.dot_general(hid[...], down_full[rows, :], (((1,), (1,)), ((), ())),
-                                    preferred_element_type=jnp.float32)
-            stage[block] = value.astype(jnp.bfloat16)
-            for d in range(1, K):
-                part_copy(d, block).start()
-        loop(0, G, group)
-
-    def lower_ring(s):
+    def lower(origin_a, gi):
+        settle(1, origin_a, gi)
+        g = (gr + gi) % G
+        block = origin_a * G + g
+        rows = pl.ds(pl.multiple_of(g * (F * R) + origin_a * (2 * R), 2 * R), 2 * R)
+        value = lax.dot_general(hid[...], down_full[rows, :], (((1,), (1,)), ((), ())),
+                                preferred_element_type=jnp.float32)
+        stage[block] = value.astype(jnp.bfloat16)
+        part[K - 1, block] = stage[block, mine]
+        for d in range(1, K):
+            part_copy(d, block).start()
+
+    def lower_ring(s, low=0, high=G):
         @pl.when(a - 1 - s >= 0)
         def _():
-            lower(a - 1 - s)
+            loop(low, high, lambda i: lower(a - 1 - s, G - 1 - i))
 
         @pl.when(a + 1 + s < A)
         def _():
-            lower(a + 1 + s)
-
-    lower(a)
-    loop(1, A - 1, lambda s: line(1, s, between=lambda: lower_ring(s - 1)))
-    lower_ring(A - 2)
-
-    for block in range(A * G):
-        total = stage[block, mine].astype(jnp.float32)
-        for d in range(1, K):
+            loop(low, high, lambda i: lower(a + 1 + s, G - 1 - i))
+
+    loop(0, G, lambda i: lower(a, G - 1 - i))
+    loop(1, A - 2, lambda s: line(1, s, between=lambda: lower_ring(s - 1)))
+    line(1, A - 2, between=lambda: lower_ring(A - 3), eager=lambda: lower_ring(A - 2, 0, G - 1))
+    lower_ring(A - 2, G - 1, G)
+
+    for d in range(1, K):
+        def landed(block):
             there = part.at[d - 1, block]
             pltpu.make_async_copy(there, there, part_recv.at[d - 1, block]).wait()
-            total += part[d - 1, block].astype(jnp.float32)
-        begin = (block % G) * (F * R) + (block // G) * (2 * R)
-        out_ref[:, begin:begin + 2 * R] = total.astype(jnp.bfloat16)
+        loop(0, A * G, landed)
 
     def drain(block):
         for d in range(1, K):
@@ -306,6 +313,29 @@
         loop(0, A - 1, lambda s: line(m, s, True))
 
 
+def finish(G, F, up_held, down_held, parts, up_out, down_out, out_ref, sems):
+    def out(m, i):
+        source, target = ((up_held, up_out), (down_held, down_out))[m]
+        size = source.shape[0] // SPLIT
+        rows = pl.ds(i * size, size)
+        return pltpu.make_async_copy(source.at[rows], target.at[rows], sems.at[m, i])
+
+    for m in range(2):
+        for i in range(SPLIT):
+            out(m, i).start()
+    K, blocks, _, wide = parts.shape
+    D = out_ref.shape[1]
+    for block in range(blocks):
+        total = parts[0, block].astype(jnp.float32)
+        for i in range(1, K):
+            total += parts[i, block].astype(jnp.float32)
+        begin = (block % G) * (D // G) + (block // G) * wide
+        out_ref[:, begin:begin + wide] = total.astype(jnp.bfloat16)
+    for m in range(2):
+        for i in range(SPLIT):
+            out(m, i).wait()
+
+
 def body(G, F, T, prompt_tokens, up_master, down_master, norm_gain):
     R, width = up_master.shape
     tok = prompt_tokens.shape[0]
@@ -317,13 +347,13 @@
     any_space = pl.BlockSpec(memory_space=pl.ANY)
     vmem_space = pl.BlockSpec(memory_space=pltpu.VMEM)
     dma = pltpu.SemaphoreType.DMA
-    return pl.pallas_call(
+    up_held, down_held, parts = pl.pallas_call(
         functools.partial(kernel, G, F, T),
         name="handoff",
         out_shape=(
             pltpu.MemorySpace.VMEM((D, W), bf16),
             pltpu.MemorySpace.VMEM((D, W), bf16),
-            jax.ShapeDtypeStruct((tok, D), bf16),
+            pltpu.MemorySpace.VMEM((K, A * G, tok, 2 * R), bf16),
         ),
         in_specs=[any_space, vmem_space, any_space, any_space],
         out_specs=(vmem_space,) * 3,
@@ -334,14 +364,26 @@
             pltpu.VMEM((K * tok, D), bf16),
             pltpu.VMEM((K * tok, W), bf16),
             pltpu.VMEM((A * G, K * tok, 2 * R), bf16),
-            pltpu.VMEM((K - 1, A * G, tok, 2 * R), bf16),
             dma((2, F, NQ)), dma((2, F, NQ)), dma((2, F, NQ)), dma((2, F, NQ)),
             dma((2, G, C)), dma((K - 1,)), dma((K - 1,)),
             dma((K - 1, A * G)), dma((K - 1, A * G)), dma((1,)), dma((2, C)),
         ],
         compiler_params=pltpu.CompilerParams(
-            collective_id=0, has_side_effects=True, vmem_limit_bytes=43 * 1024 * 1024),
+            collective_id=0, has_side_effects=True, vmem_limit_bytes=41 * 1024 * 1024),
     )(prompt_tokens, norm_gain.reshape(1, R), up_master, down_master)
+    return pl.pallas_call(
+        functools.partial(finish, G, F),
+        name="finish",
+        out_shape=(
+            jax.ShapeDtypeStruct((D, W), bf16),
+            jax.ShapeDtypeStruct((D, W), bf16),
+            jax.ShapeDtypeStruct((tok, D), bf16),
+        ),
+        in_specs=[vmem_space] * 3,
+        out_specs=(any_space, any_space, vmem_space),
+        scratch_shapes=[dma((2, SPLIT))],
+        compiler_params=pltpu.CompilerParams(vmem_limit_bytes=16 * 1024 * 1024),
+    )(up_held, down_held, parts)
 
 
 def solution(mesh):

time: 190 us -> 192 us (1.011)
  Pallas kernels: 182 us -> 191 us
  local copies, waits for them, and re-layouts: 7.61 us -> 0 us
    unnamed x5 -> x0, local copies, waits for them, and re-layouts: 7.61 us -> none
    pallas_call x0 -> x1, Pallas kernels: none -> 6.74 us  [body(): pl.pallas_call(functools.partial(finish, G, F), name='finish', out_shape=...]
    pallas_call x1, Pallas kernels: 182 us -> 184 us  [body(): pl.pallas_call(functools.partial(kernel, G, F, T), name='handoff', out_sh...]
where the time goes in v3:
time: 192 us
  Pallas kernels  191 us (99%)
    pallas_call x1, Pallas kernels, body(): pl.pallas_call(functools.partial(kernel, G, F, T), name='handoff', out_sh...  184 us
    pallas_call x1, Pallas kernels, body(): pl.pallas_call(functools.partial(finish, G, F), name='finish', out_shape=...  6.74 us

profile of v3, /device:TPU:0, one launch (start us, length us, event | category | flops | bytes accessed | tf_op | source)
XLA Modules:
  0.0 191.8 jit_solution(6624130351364849466)
XLA Ops:
  0.6 184.4 %handoff.1 = (bf16[2048,2048]{1,0:T(8,128)(2,1)S(1)}, bf16[2048,2048]{1,0:T(8,128)(2,1)S(1)}, bf16[4,8,144,256]{3,2,1,0:T(8,128)(2,1)S(1)}) custom-call(bf16[144,2048]{1,0:T(8,128)(2,1)} %tok_in.1, f32[1,128]{1,0:T(1,128)} %bitcast.1, f32[128,4096]{1,0:T(8,128)} %up_in.1, f32[128,4096]{1,0:T(8,128)} %down_in.1), custom_call_target="tpu_custom_call" | custom-call | tf_op jit(solution)/shard_map/handoff/pallas_call | solution.py:350
  185.1 6.7 %finish.1 = (bf16[2048,2048]{1,0:T(8,128)(2,1)}, bf16[2048,2048]{1,0:T(8,128)(2,1)}, bf16[144,2048]{1,0:T(8,128)(2,1)}) custom-call(bf16[2048,2048]{1,0:T(8,128)(2,1)S(1)} %get-tuple-element.6.up_held, bf16[2048,2048]{1,0:T(8,128)(2,1)S(1)} %get-tuple-element.7.down_held, bf16[4,8,144,256]{3,2,1,0:T(8,128)(2,1)S(1)} %get-tuple-element.8.parts), custom_call_target="tpu_custom_call" | custom-call | tf_op jit(solution)/shard_map/finish/pallas_call | solution.py:374

commit v4 on v3

--- a/solution.py
+++ b/solution.py
@@ -8,7 +8,7 @@
 from jax.sharding import PartitionSpec as P
 
 MESH = pl.DeviceIdType.MESH
-CHUNK = 16
+CHUNK = 32
 TILE = 256
 SPLIT = 4
 

time: 192 us -> 185 us (0.964)
  Pallas kernels: 191 us -> 185 us
    pallas_call x1, Pallas kernels: 184 us -> 178 us  [body(): pl.pallas_call(functools.partial(kernel, G, F, T), name='handoff', out_sh...]
where the time goes in v4:
time: 185 us
  Pallas kernels  185 us (100%)
    pallas_call x1, Pallas kernels, body(): pl.pallas_call(functools.partial(kernel, G, F, T), name='handoff', out_sh...  178 us
    pallas_call x1, Pallas kernels, body(): pl.pallas_call(functools.partial(finish, G, F), name='finish', out_shape=...  6.74 us

profile of v4, /device:TPU:0, one launch (start us, length us, event | category | flops | bytes accessed | tf_op | source)
XLA Modules:
  0.0 185.2 jit_solution(7361861711681150747)
XLA Ops:
  0.6 177.9 %handoff.1 = (bf16[2048,2048]{1,0:T(8,128)(2,1)S(1)}, bf16[2048,2048]{1,0:T(8,128)(2,1)S(1)}, bf16[4,8,144,256]{3,2,1,0:T(8,128)(2,1)S(1)}) custom-call(bf16[144,2048]{1,0:T(8,128)(2,1)} %tok_in.1, f32[1,128]{1,0:T(1,128)} %bitcast.1, f32[128,4096]{1,0:T(8,128)} %up_in.1, f32[128,4096]{1,0:T(8,128)} %down_in.1), custom_call_target="tpu_custom_call" | custom-call | tf_op jit(solution)/shard_map/handoff/pallas_call | solution.py:350
  178.5 6.7 %finish.1 = (bf16[2048,2048]{1,0:T(8,128)(2,1)}, bf16[2048,2048]{1,0:T(8,128)(2,1)}, bf16[144,2048]{1,0:T(8,128)(2,1)}) custom-call(bf16[2048,2048]{1,0:T(8,128)(2,1)S(1)} %get-tuple-element.6.up_held, bf16[2048,2048]{1,0:T(8,128)(2,1)S(1)} %get-tuple-element.7.down_held, bf16[4,8,144,256]{3,2,1,0:T(8,128)(2,1)S(1)} %get-tuple-element.8.parts), custom_call_target="tpu_custom_call" | custom-call | tf_op jit(solution)/shard_map/finish/pallas_call | solution.py:374
